TPU v7x, 128 devices: a whole 4x4x4 slice. The times are simulated.
128 devices in a mesh: sp: 16 (over z, y), tp: 8 (over x, core).
Axes of the slice: x: 4, y: 4, z: 4, core: 2. Of those that a mesh axis runs over, the one named last changes fastest.
Arguments:
- inputs: bfloat16 [16384, 2048], P(('sp', 'tp')), may hold values from -90 to 90
- in_gain: float32 [2048], replicated, may hold values from 0.1 to 1.9
- w_query: bfloat16 [2048, 1024], replicated, may hold values from -2 to 2
- w_key: bfloat16 [2048, 128], replicated, may hold values from -2 to 2
- w_value: bfloat16 [2048, 128], replicated, may hold values from -0.125 to 0.125
- query_gain: float32 [64], replicated, may hold values from 0 to 8, as said below
- key_gain: float32 [64], replicated, may hold values from 0 to 8, as said below
- decay_sums: float32 [16384, 16], P('sp', 'tp'), may hold values from -2343 to 0, as said below
- w_out: bfloat16 [1024, 2048], replicated, may hold values from -0.1875 to 0.1875
Outputs:
- result: bfloat16 [16384, 2048], P(('sp', 'tp'))
Inputs may be any that keep to these rules, and one draw needn't show every extreme that they name: `decay_sums`: along positions, each head's entries never rise. `query_gain`: every entry is positive. `key_gain`: every entry is positive.
All inputs are finite; a program needn't handle non-finite values.
Results may differ from a plain program's by a relative error of at most 0.015.
The roundings to bfloat16 on the way count: a program that leaves them out, or rounds other values in their place, can miss the bound.
Values may be sent and summed in bfloat16 or wider, within the bound.
A program may use at most 64 MiB of HBM per device.

v0:
```python
from functools import partial
import math
import jax
import jax.numpy as jnp
from jax import lax
from jax.sharding import Mesh
from jax.sharding import PartitionSpec as P

TP = ("tp_0", "tp_1")
SP_TP = ("sp", "tp_0", "tp_1")
epsilon = 1e-06


def joined_along(tiles, dim):
    tiles = jnp.moveaxis(tiles, 0, dim)
    lengths = tiles.shape
    return tiles.reshape(*lengths[:dim], lengths[dim] * lengths[dim + 1], *lengths[dim + 2 :])


def from_everyone(value, axis):
    length = lax.axis_size(axis)
    return lax.all_to_all(
        jnp.broadcast_to(value[None], (length, *value.shape)), axis, 0, 0, tiled=True
    )


def gathered_copies(value, axis, dim):
    return joined_along(from_everyone(value, axis), dim)


def partner(value, axis, stride):
    return lax.ppermute(value, axis, [(i, i ^ 1 << stride) for i in range(lax.axis_size(axis))])


def cut_along(value, dim, length):
    before, after = (value.shape[:dim], value.shape[dim + 1 :])
    return jnp.moveaxis(value.reshape(*before, length, -1, *after), dim, 0)


def moved_by_axis(tiles, axes, sequence):
    inside = tiles.shape[1:]
    filled = tiles.reshape(*(lax.axis_size(a) for a in axes), *inside)
    for k in sequence:
        filled = lax.all_to_all(filled, axes[k], k, k, tiled=True)
    return filled.reshape(-1, *inside)


def stepwise_exchange(value, axes, sequence, split_dim, concat_dim):
    tiles = cut_along(value, split_dim, lax.axis_size(axes))
    return joined_along(moved_by_axis(tiles, axes, sequence), concat_dim)


def rms_norm(vector, gain_vec):
    return (
        vector * lax.rsqrt(jnp.mean(vector * vector, axis=-1, keepdims=True) + epsilon) * gain_vec
    )


def attend_step(
    masked, query_rows, query_decay, query_pos, key_slice, value_slice, decay_slice, key_pos, inner
):
    peak, total, weighted = inner
    score_scale = query_rows.shape[2] ** (-0.5)
    scores = (
        jnp.einsum("thd,ud->htu", query_rows, key_slice, preferred_element_type=jnp.float32)
        * score_scale
    )
    scores = scores + query_decay[:, :, None] - decay_slice[:, None, :]
    if masked:
        visible = key_pos[None, :] <= query_pos[:, None]
        scores = jnp.where(visible[None], scores, -1e30)
    peak_new = jnp.maximum(peak, jnp.max(scores, axis=-1))
    weights_exp = jnp.exp(scores - peak_new[:, :, None])
    if masked:
        weights_exp = jnp.where(visible[None], weights_exp, 0.0)
    rescale = jnp.exp(peak - peak_new)
    total_new = total * rescale + jnp.sum(weights_exp, axis=-1)
    product = jnp.einsum(
        "htu,ud->thd",
        weights_exp.astype(jnp.bfloat16),
        value_slice,
        preferred_element_type=jnp.float32,
    )
    weighted_new = weighted * rescale.T[:, :, None] + product
    return (peak_new, total_new, weighted_new)


def keep_state(inner):
    return inner


def per_device(inputs, in_gain, w_query, w_key, w_value, query_gain, key_gain, decay_sums, w_out):
    tp_count = lax.axis_size(TP)
    sp_count = lax.axis_size("sp")
    sp_rank = lax.axis_index("sp")
    heads_dev = decay_sums.shape[1]
    head_size = query_gain.shape[0]
    kv_heads = w_key.shape[1] // head_size
    width_dev = heads_dev * head_size
    normed = rms_norm(inputs.astype(jnp.float32), in_gain).astype(jnp.bfloat16)
    row_count = normed.shape[0]
    all_heads = w_query.shape[1] // head_size
    query_all = rms_norm(
        jnp.dot(normed, w_query, preferred_element_type=jnp.float32).reshape(
            row_count, all_heads, head_size
        ),
        query_gain,
    ).astype(jnp.bfloat16)
    key_all = rms_norm(
        jnp.dot(normed, w_key, preferred_element_type=jnp.float32).reshape(
            row_count, kv_heads, head_size
        ),
        key_gain,
    ).astype(jnp.bfloat16)
    value_all = (
        jnp.dot(normed, w_value, preferred_element_type=jnp.float32)
        .astype(jnp.bfloat16)
        .reshape(row_count, kv_heads, head_size)
    )
    pair_all = jnp.repeat(
        jnp.concatenate([key_all, value_all], axis=2), tp_count // kv_heads, axis=1
    )
    packed = jnp.concatenate([query_all.reshape(row_count, tp_count, width_dev), pair_all], axis=2)
    received = lax.all_to_all(packed, TP, split_axis=1, concat_axis=0, tiled=True)[:, 0]
    tok_rows = received.shape[0]
    queries = received[:, :width_dev].reshape(tok_rows, heads_dev, head_size)
    key_values = received[:, width_dev:]
    all_decays = gathered_copies(decay_sums, "sp", 0)
    half_rows = tok_rows // 2
    bit_steps = sp_count.bit_length() - 1
    far_queries = queries[half_rows:]
    for bit in range(bit_steps):
        far_queries = partner(far_queries, "sp", bit)
    mirror = sp_count - 1 - sp_rank
    groups = [
        (queries[:half_rows], sp_rank * tok_rows),
        (far_queries, mirror * tok_rows + half_rows),
    ]
    prepared = []
    for query_rows, first_pos in groups:
        rows = query_rows.shape[0]
        query_decay = lax.dynamic_slice_in_dim(all_decays, first_pos, rows, 0).T
        query_pos = first_pos + jnp.arange(rows, dtype=jnp.int32)
        prepared.append((query_rows, query_decay, query_pos, first_pos, first_pos + rows - 1))
    initial = tuple(
        (
            (
                jnp.full((heads_dev, entry[0].shape[0]), -1e30, jnp.float32),
                jnp.zeros((heads_dev, entry[0].shape[0]), jnp.float32),
                jnp.zeros((entry[0].shape[0], heads_dev, head_size), jnp.float32),
            )
            for entry in prepared
        )
    )
    state = initial
    pieces = lax.all_gather(key_values, "sp", axis=0, tiled=True)
    piece_rows = pieces.shape[0]
    key_block = math.gcd(piece_rows, 512)

    def one_block(carry, block_index):
        key_start = block_index * key_block
        pair_slice = lax.dynamic_slice_in_dim(pieces, block_index * key_block, key_block, 0)
        key_slice = pair_slice[:, :head_size]
        value_slice = pair_slice[:, head_size:]
        decay_slice = lax.dynamic_slice_in_dim(all_decays, key_start, key_block, 0).T
        key_pos = key_start + jnp.arange(key_block, dtype=jnp.int32)
        updated = []
        for (query_rows, query_decay, query_pos, first_pos, last_pos), inner in zip(
            prepared, carry
        ):
            branch = jnp.where(
                key_start > last_pos, 0, jnp.where(key_start + key_block - 1 <= first_pos, 1, 2)
            )
            full_step = partial(
                attend_step,
                False,
                query_rows,
                query_decay,
                query_pos,
                key_slice,
                value_slice,
                decay_slice,
                key_pos,
            )
            masked_step = partial(
                attend_step,
                True,
                query_rows,
                query_decay,
                query_pos,
                key_slice,
                value_slice,
                decay_slice,
                key_pos,
            )
            updated.append(lax.switch(branch, [keep_state, full_step, masked_step], inner))
        return (tuple(updated), None)

    state, unused = lax.scan(one_block, state, jnp.arange(piece_rows // key_block, dtype=jnp.int32))
    outputs = [
        (weighted / total.T[:, :, None]).astype(jnp.bfloat16) for peak, total, weighted in state
    ]
    returned = outputs[1]
    for bit in range(bit_steps):
        returned = partner(returned, "sp", bit)
    attended = jnp.concatenate([outputs[0], returned], axis=0).reshape(tok_rows, width_dev)
    out_rows = stepwise_exchange(attended, TP, (1, 0), 0, 1)
    result = jnp.dot(out_rows, w_out, preferred_element_type=jnp.float32).astype(jnp.bfloat16)
    return result


def solution(mesh):
    torus = Mesh(mesh.devices.reshape(mesh.shape["sp"], 4, 2), ("sp", "tp_0", "tp_1"))
    in_specs = (P(SP_TP, None), P(), P(), P(), P(), P(), P(), P("sp", TP), P())
    out_specs = P(SP_TP, None)
    return jax.shard_map(
        per_device, mesh=torus, in_specs=in_specs, out_specs=out_specs, check_vma=False
    )
```

profile of v0, /device:TPU:24, one launch (start us, length us, event | category | flops | bytes accessed | tf_op | source)
XLA Modules:
  0.0 267.5 jit_solution(12323590933669240431)
XLA Ops:
  7.9 1.5 multiply_reduce_fusion
  9.4 1.6 convolution_convert_fusion.1
  11.0 3.0 %fusion.64 = (f32[128,1024]{1,0:T(8,128)S(1)}, f32[128,1024]{1,0:T(8,128)S(1)}) fusion(bf16[2048,1024]{1,0:T(8,128)(2,1)} %param.19, bf16[128,2048]{1,0:T(8,128)(2,1)S(1)} %copy-done.1, f32[2048]{0:T(1024)S(1)} %copy-done.2, f32[128]{0:T(128)S(1)} %add_rsqrt_fusion.2), kind=kOutput, calls=%fused_computation.100 | convolution fusion | flops 538050560 | bytes 5775872 | tf_op jit(solution)/shard_map/dot_general | solution.py:104
  15.1 14.5 %all_to_all.30 = bf16[128,8,256]{0,2,1:T(8,128)(2,1)S(1)} all-to-all(bf16[128,8,256]{0,2,1:T(8,128)(2,1)S(1)} %pad_maximum_fusion), channel_id=1, replica_groups=mesh['sp'=16,'tp_0'=4,'tp_1'=2] {'tp_0','tp_1'}, dimensions={1} | all-to-all | bytes 1048576 | tf_op jit(solution)/shard_map/all_to_all | solution.py:124
  31.5 4.3 %collective-permute-done = bf16[512,2,64]{0,2,1:T(8,128)(2,1)S(1)} collective-permute-done((bf16[512,2,64]{0,2,1:T(8,128)(2,1)S(1)}, bf16[512,2,64]{0,2,1:T(8,128)(2,1)S(1)}, u32[]{:S(2)}, u32[]{:S(2)}) %collective-permute-start) | collective-permute-done | bytes 131104 | tf_op jit(solution)/shard_map/ppermute | solution.py:32
  36.9 5.3 %collective-permute-done.1 = bf16[512,2,64]{0,2,1:T(8,128)(2,1)S(1)} collective-permute-done((bf16[512,2,64]{0,2,1:T(8,128)(2,1)S(1)}, bf16[512,2,64]{0,2,1:T(8,128)(2,1)S(1)}, u32[]{:S(2)}, u32[]{:S(2)}) %collective-permute-start.1) | collective-permute-done | bytes 131104 | tf_op jit(solution)/shard_map/ppermute | solution.py:32
  42.2 1.9 collective-permute-start.2
  44.8 8.9 %all-to-all-start.1 = ((f32[16,1024,2]{1,2,0:T(2,128)}), f32[16,1024,2]{1,2,0:T(2,128)S(1)}, u32[]{:S(2)}, u32[]{:S(2)}) async-start(f32[16,1024,2]{1,2,0:T(2,128)} %broadcast_in_dim.53), calls=%async_computation.1 | async-start | bytes 262144 | tf_op jit(solution)/shard_map/all_to_all | solution.py:22
  53.7 3.1 %collective-permute-start.3 = (bf16[512,2,64]{0,2,1:T(8,128)(2,1)S(1)}, bf16[512,2,64]{0,2,1:T(8,128)(2,1)S(1)}, u32[]{:S(2)}, u32[]{:S(2)}) collective-permute-start(bf16[512,2,64]{0,2,1:T(8,128)(2,1)S(1)} %collective-permute-done.2), channel_id=1, source_target_pairs={{0,64},{8,72},{16,80},{24,88},{32,96},{40,104},{48,112},{56,120},{... | collective-permute-start | bytes 393224 | tf_op jit(solution)/shard_map/ppermute | solution.py:32
  56.7 2.7 %all-to-all-done.1 = f32[16,1024,2]{1,2,0:T(2,128)S(1)} async-done(((f32[16,1024,2]{1,2,0:T(2,128)}), f32[16,1024,2]{1,2,0:T(2,128)S(1)}, u32[]{:S(2)}, u32[]{:S(2)}) %all-to-all-start.1) | async-done | bytes 131104 | tf_op jit(solution)/shard_map/all_to_all | solution.py:22
  60.6 23.3 %all-gather.2.cloned.1.call-done = bf16[16384,128]{1,0:T(8,128)(2,1)} async-done(((bf16[1024,128]{1,0:T(8,128)(2,1)}), bf16[16384,128]{1,0:T(8,128)(2,1)}) %all-gather.2.cloned.1.call-update) | async-done | bytes 4194320 | tf_op jit(solution)/shard_map/all_gather | solution.py:156
  84.0 133.3 %while.26 = (s32[]{:T(128)}, f32[2,512]{1,0:T(2,128)S(1)}, f32[2,512]{1,0:T(2,128)S(1)}, f32[512,2,64]{0,2,1:T(8,128)S(1)}, f32[2,512]{1,0:T(2,128)S(1)}, /*inde...) while((s32[]{:T(128)}, f32[2,512]{1,0:T(2,128)S(1)}, ...), condition=%wide.region_18.19_spmd.clone.clone, body=%wide.region_3.18_spmd.clone.clone.sunk | while | flops 280763904 | bytes 16956256 | solution.py:199
  99.0 1.4 conditional.8
  104.4 1.4 conditional.8
  120.8 2.1 conditional.8
  199.0 2.1 conditional.9
  218.3 4.2 %collective-permute-done.4 = bf16[512,2,64]{0,2,1:T(8,128)(2,1)S(1)} collective-permute-done((bf16[512,2,64]{0,2,1:T(8,128)(2,1)S(1)}, bf16[512,2,64]{0,2,1:T(8,128)(2,1)S(1)}, u32[]{:S(2)}, u32[]{:S(2)}) %collective-permute-start.4) | collective-permute-done | bytes 131104 | tf_op jit(solution)/shard_map/ppermute | solution.py:32
  222.5 1.4 collective-permute-start.5
  223.9 5.1 %collective-permute-done.5 = bf16[512,2,64]{0,2,1:T(8,128)(2,1)S(1)} collective-permute-done((bf16[512,2,64]{0,2,1:T(8,128)(2,1)S(1)}, bf16[512,2,64]{0,2,1:T(8,128)(2,1)S(1)}, u32[]{:S(2)}, u32[]{:S(2)}) %collective-permute-start.5) | collective-permute-done | bytes 131104 | tf_op jit(solution)/shard_map/ppermute | solution.py:32
  229.2 6.0 %collective-permute-done.6 = bf16[512,2,64]{0,2,1:T(8,128)(2,1)S(1)} collective-permute-done((bf16[512,2,64]{0,2,1:T(8,128)(2,1)S(1)}, bf16[512,2,64]{0,2,1:T(8,128)(2,1)S(1)}, u32[]{:S(2)}, u32[]{:S(2)}) %collective-permute-start.6) | collective-permute-done | bytes 131104 | tf_op jit(solution)/shard_map/ppermute | solution.py:32
  235.5 6.2 %collective-permute-done.7 = bf16[512,2,64]{0,2,1:T(8,128)(2,1)S(1)} collective-permute-done((bf16[512,2,64]{0,2,1:T(8,128)(2,1)S(1)}, bf16[512,2,64]{0,2,1:T(8,128)(2,1)S(1)}, u32[]{:S(2)}, u32[]{:S(2)}) %collective-permute-start.7) | collective-permute-done | bytes 131104 | tf_op jit(solution)/shard_map/ppermute | solution.py:32
  241.9 3.9 %all_to_all.31 = bf16[4,2,128,128]{2,3,0,1:T(8,128)(2,1)S(1)} all-to-all(bf16[4,2,128,128]{2,3,0,1:T(8,128)(2,1)S(1)} %copy.78), channel_id=1, replica_groups=mesh['sp'=16,'tp_0'=4,'tp_1'=2] {'tp_1'}, dimensions={1} | all-to-all | bytes 524288 | tf_op jit(solution)/shard_map/all_to_all | solution.py:44
  245.9 11.1 %all_to_all.32 = bf16[4,2,128,128]{2,3,1,0:T(8,128)(2,1)S(1)} all-to-all(bf16[4,2,128,128]{2,3,1,0:T(8,128)(2,1)S(1)} %copy.79), channel_id=1, replica_groups=mesh['sp'=16,'tp_0'=4,'tp_1'=2] {'tp_0'}, dimensions={0} | all-to-all | bytes 524288 | tf_op jit(solution)/shard_map/all_to_all | solution.py:44
  256.9 3.7 %convolution_convert_fusion = bf16[128,2048]{1,0:T(8,128)(2,1)} fusion(bf16[128,1024]{0,1:T(8,128)(2,1)S(1)} %bitcast.133, bf16[1024,2048]{1,0:T(8,128)(2,1)} %param.25), kind=kOutput, calls=%fused_computation.69 | convolution fusion | flops 537133056 | bytes 4980736 | tf_op jit(solution)/shard_map/dot_general | solution.py:208
  (574 shorter events, 155.9 us)
Async XLA Ops:
  6.5 1.3 copy-start
  6.5 4.4 %copy-start.1 = (bf16[128,2048]{1,0:T(8,128)(2,1)S(1)}, bf16[128,2048]{1,0:T(8,128)(2,1)}, u32[]{:S(2)}) copy-start(bf16[128,2048]{1,0:T(8,128)(2,1)} %param.17) | copy-start | bytes 1572868
  6.5 4.5 %copy-start.2 = (f32[2048]{0:T(1024)S(1)}, f32[2048]{0:T(1024)}, u32[]{:S(2)}) copy-start(f32[2048]{0:T(1024)} %param.18) | copy-start | bytes 24580
  6.5 77.4 %all-gather.2.cloned.1.call-start = ((), (), s32[]{:S(2)}) async-start(), calls=%async_computation.4 | async-start | bytes 4456448 | tf_op jit(solution)/shard_map/all_gather | solution.py:156
  14.0 0.7 copy-start.5
  14.0 0.7 copy-start.4
  15.1 29.1 %copy-start.3 = (f32[1024,2]{0,1:T(2,128)S(1)}, f32[1024,2]{0,1:T(2,128)}, u32[]{:S(2)}) copy-start(f32[1024,2]{0,1:T(2,128)} %param.24) | copy-start | bytes 24580
  30.6 5.1 %collective-permute-start = (bf16[512,2,64]{0,2,1:T(8,128)(2,1)S(1)}, bf16[512,2,64]{0,2,1:T(8,128)(2,1)S(1)}, u32[]{:S(2)}, u32[]{:S(2)}) collective-permute-start(bf16[512,2,64]{0,2,1:T(8,128)(2,1)S(1)} %bitcast.139), channel_id=1, source_target_pairs={{0,8},{8,0},{16,24},{24,16},{32,40},{40,32},{48,56},{56,48},{64,72... | collective-permute-start | bytes 393224 | tf_op jit(solution)/shard_map/ppermute | solution.py:32
  35.7 6.5 %collective-permute-start.1 = (bf16[512,2,64]{0,2,1:T(8,128)(2,1)S(1)}, bf16[512,2,64]{0,2,1:T(8,128)(2,1)S(1)}, u32[]{:S(2)}, u32[]{:S(2)}) collective-permute-start(bf16[512,2,64]{0,2,1:T(8,128)(2,1)S(1)} %collective-permute-done), channel_id=1, source_target_pairs={{0,16},{8,24},{16,0},{24,8},{32,48},{40,56},{48,32},{56,40},{64,80... | collective-permute-start | bytes 393224 | tf_op jit(solution)/shard_map/ppermute | solution.py:32
  42.2 11.5 %collective-permute-start.2 = (bf16[512,2,64]{0,2,1:T(8,128)(2,1)S(1)}, bf16[512,2,64]{0,2,1:T(8,128)(2,1)S(1)}, u32[]{:S(2)}, u32[]{:S(2)}) collective-permute-start(bf16[512,2,64]{0,2,1:T(8,128)(2,1)S(1)} %collective-permute-done.1), channel_id=1, source_target_pairs={{0,32},{8,40},{16,48},{24,56},{32,0},{40,8},{48,16},{56,24},{64,96... | collective-permute-start | bytes 393224 | tf_op jit(solution)/shard_map/ppermute | solution.py:32
  44.8 14.6 %all-to-all-start.1 = ((f32[16,1024,2]{1,2,0:T(2,128)}), f32[16,1024,2]{1,2,0:T(2,128)S(1)}, u32[]{:S(2)}, u32[]{:S(2)}) async-start(f32[16,1024,2]{1,2,0:T(2,128)} %broadcast_in_dim.53), calls=%async_computation.1 | async-start | bytes 262144 | tf_op jit(solution)/shard_map/all_to_all | solution.py:22
  53.7 6.9 %collective-permute-start.3 = (bf16[512,2,64]{0,2,1:T(8,128)(2,1)S(1)}, bf16[512,2,64]{0,2,1:T(8,128)(2,1)S(1)}, u32[]{:S(2)}, u32[]{:S(2)}) collective-permute-start(bf16[512,2,64]{0,2,1:T(8,128)(2,1)S(1)} %collective-permute-done.2), channel_id=1, source_target_pairs={{0,64},{8,72},{16,80},{24,88},{32,96},{40,104},{48,112},{56,120},{... | collective-permute-start | bytes 393224 | tf_op jit(solution)/shard_map/ppermute | solution.py:32
  217.4 5.1 %collective-permute-start.4 = (bf16[512,2,64]{0,2,1:T(8,128)(2,1)S(1)}, bf16[512,2,64]{0,2,1:T(8,128)(2,1)S(1)}, u32[]{:S(2)}, u32[]{:S(2)}) collective-permute-start(bf16[512,2,64]{0,2,1:T(8,128)(2,1)S(1)} %divide_convert_fusion), channel_id=1, source_target_pairs={{0,8},{8,0},{16,24},{24,16},{32,40},{40,32},{48,56},{56,48},{64,72... | collective-permute-start | bytes 393224 | tf_op jit(solution)/shard_map/ppermute | solution.py:32
  222.5 6.5 %collective-permute-start.5 = (bf16[512,2,64]{0,2,1:T(8,128)(2,1)S(1)}, bf16[512,2,64]{0,2,1:T(8,128)(2,1)S(1)}, u32[]{:S(2)}, u32[]{:S(2)}) collective-permute-start(bf16[512,2,64]{0,2,1:T(8,128)(2,1)S(1)} %collective-permute-done.4), channel_id=1, source_target_pairs={{0,16},{8,24},{16,0},{24,8},{32,48},{40,56},{48,32},{56,40},{64,80... | collective-permute-start | bytes 393224 | tf_op jit(solution)/shard_map/ppermute | solution.py:32
  229.0 6.2 %collective-permute-start.6 = (bf16[512,2,64]{0,2,1:T(8,128)(2,1)S(1)}, bf16[512,2,64]{0,2,1:T(8,128)(2,1)S(1)}, u32[]{:S(2)}, u32[]{:S(2)}) collective-permute-start(bf16[512,2,64]{0,2,1:T(8,128)(2,1)S(1)} %collective-permute-done.5), channel_id=1, source_target_pairs={{0,32},{8,40},{16,48},{24,56},{32,0},{40,8},{48,16},{56,24},{64,96... | collective-permute-start | bytes 393224 | tf_op jit(solution)/shard_map/ppermute | solution.py:32
  235.2 6.5 %collective-permute-start.7 = (bf16[512,2,64]{0,2,1:T(8,128)(2,1)S(1)}, bf16[512,2,64]{0,2,1:T(8,128)(2,1)S(1)}, u32[]{:S(2)}, u32[]{:S(2)}) collective-permute-start(bf16[512,2,64]{0,2,1:T(8,128)(2,1)S(1)} %collective-permute-done.6), channel_id=1, source_target_pairs={{0,64},{8,72},{16,80},{24,88},{32,96},{40,104},{48,112},{56,120},{... | collective-permute-start | bytes 393224 | tf_op jit(solution)/shard_map/ppermute | solution.py:32
Sparse Core Ops, SparseCore 0:
  30.6 53.2 all-gather.1
where the time goes:
time: 269 us; the launch traced here: 268 us
  local copies, waits for them, and re-layouts  63.6 us (24%)
  waiting for transfers between devices  58.1 us (22%)
  matrix products  43.4 us (16%)
  blocking collectives  29.4 us (11%)
  loops' own time  27.2 us (10%)
  starting transfers between devices  18.6 us (7%)
  between operations  13.7 us (5%)
  other arithmetic  13.4 us (5%)
    slice x32, local copies, waits for them, and re-layouts, one_block(): value_slice = pair_slice[:, head_size:]  35.1 us
    ppermute x8, waiting for transfers between devices, partner(): lax.ppermute(value, axis, [(i, i ^ 1 << stride) for i in range(lax.axis_s...  32 us
    another operation x1, loops' own time, per_device(): lax.scan(one_block, state, jnp.arange(piece_rows // key_block, dtype=jnp....  24.6 us
    all_gather x1, waiting for transfers between devices, per_device(): pieces = lax.all_gather(key_values, 'sp', axis=0, tiled=True)  23.3 us
    dynamic_slice x32, local copies, waits for them, and re-layouts, per_device(): lax.scan(one_block, state, jnp.arange(piece_rows // key_block, dtype=jnp....  18.8 us
    dot_general x33, matrix products, attend_step(): jnp.einsum('htu,ud->thd', weights_exp.astype(jnp.bfloat16), value_slice,...  17.1 us
    dot_general x33, matrix products, attend_step(): jnp.einsum('thd,ud->htu', query_rows, key_slice, preferred_element_type=j...  16.6 us
    all_to_all x2, blocking collectives, moved_by_axis(): filled = lax.all_to_all(filled, axes[k], k, k, tiled=True)  15 us
  transfers between devices with their start and end apart: 10, of which 9 were waited for; matrix products, arithmetic and copies ran while one was open for 0% of the time, Pallas kernels for 0%

commit v1 on v0

--- a/solution.py
+++ b/solution.py
@@ -153,7 +153,10 @@
         )
     )
     state = initial
-    pieces = lax.all_gather(key_values, "sp", axis=0, tiled=True)
+    size = lax.axis_size("sp")
+    blocks = jnp.stack([key_values for _ in range(size)])
+    blocks = lax.all_to_all(blocks, "sp", split_axis=0, concat_axis=0)
+    pieces = jnp.concatenate(blocks, axis=0)
     piece_rows = pieces.shape[0]
     key_block = math.gcd(piece_rows, 512)
 

time: 269 us -> 304 us (1.13)
  waiting for transfers between devices: 58.1 us -> 98.2 us
  between operations: 13.7 us -> 0.3 us
  local copies, waits for them, and re-layouts: 63.6 us -> 73 us
    ppermute x8, waiting for transfers between devices: 32 us -> 92.8 us  [partner(): lax.ppermute(value, axis, [(i, i ^ 1 << stride) for i in range(lax.axis_s...]
    all_gather x1 -> x0, waiting for transfers between devices: 23.3 us -> none  [per_device(): pieces = lax.all_gather(key_values, 'sp', axis=0, tiled=True)]
    all_to_all x0 -> x1, starting transfers between devices: none -> 6.59 us  [per_device(): blocks = lax.all_to_all(blocks, 'sp', split_axis=0, concat_axis=0)]
    all_to_all x0 -> x1, local copies, waits for them, and re-layouts: none -> 6.39 us  [per_device(): blocks = lax.all_to_all(blocks, 'sp', split_axis=0, concat_axis=0)]
    ppermute x8, starting transfers between devices: 9.74 us -> 4.91 us  [partner(): lax.ppermute(value, axis, [(i, i ^ 1 << stride) for i in range(lax.axis_s...]
  transfers between devices with their start and end apart: 10 -> 10, of which waited for: 9 -> 8; matrix products, arithmetic and copies ran while one was open for 0% -> 2% of each run, Pallas kernels for 0% -> 0%
where the time goes in v1:
time: 304 us; the launch traced here: 302 us
  waiting for transfers between devices  98.2 us (32%)
  local copies, waits for them, and re-layouts  73 us (24%)
  matrix products  43.4 us (14%)
  blocking collectives  28 us (9%)
  loops' own time  25.9 us (9%)
  starting transfers between devices  19.7 us (6%)
  other arithmetic  13.5 us (4%)
    ppermute x8, waiting for transfers between devices, partner(): lax.ppermute(value, axis, [(i, i ^ 1 << stride) for i in range(lax.axis_s...  92.8 us
    slice x32, local copies, waits for them, and re-layouts, one_block(): value_slice = pair_slice[:, head_size:]  35.2 us
    another operation x1, loops' own time, per_device(): lax.scan(one_block, state, jnp.arange(piece_rows // key_block, dtype=jnp....  23.4 us
    dynamic_slice x32, local copies, waits for them, and re-layouts, per_device(): lax.scan(one_block, state, jnp.arange(piece_rows // key_block, dtype=jnp....  19.8 us
    dot_general x33, matrix products, attend_step(): jnp.einsum('htu,ud->thd', weights_exp.astype(jnp.bfloat16), value_slice,...  17 us
    dot_general x33, matrix products, attend_step(): jnp.einsum('thd,ud->htu', query_rows, key_slice, preferred_element_type=j...  16.6 us
    all_to_all x1, blocking collectives, per_device(): lax.all_to_all(packed, TP, split_axis=1, concat_axis=0, tiled=True)[:, 0]  14.5 us
    all_to_all x2, blocking collectives, moved_by_axis(): filled = lax.all_to_all(filled, axes[k], k, k, tiled=True)  13.6 us
  transfers between devices with their start and end apart: 10, of which 8 were waited for; matrix products, arithmetic and copies ran while one was open for 2% of the time, Pallas kernels for 0%

profile of v1, /device:TPU:24, one launch (start us, length us, event | category | flops | bytes accessed | tf_op | source)
XLA Modules:
  0.0 302.0 jit_solution(18164895993497804181)
XLA Ops:
  1.3 1.5 multiply_reduce_fusion
  2.8 1.6 convolution_convert_fusion.1
  4.5 3.0 fusion.64
  8.6 14.5 %all_to_all.35 = bf16[128,8,256]{0,2,1:T(8,128)(2,1)S(1)} all-to-all(bf16[128,8,256]{0,2,1:T(8,128)(2,1)S(1)} %pad_maximum_fusion), channel_id=1, replica_groups=mesh['sp'=16,'tp_0'=4,'tp_1'=2] {'tp_0','tp_1'}, dimensions={1} | all-to-all | bytes 1048576 | tf_op jit(solution)/shard_map/all_to_all | solution.py:124
  23.7 8.2 %all-to-all-start.2 = ((f32[16,1024,2]{1,2,0:T(2,128)}), f32[16,1024,2]{1,2,0:T(2,128)S(1)}, u32[]{:S(2)}, u32[]{:S(2)}) async-start(f32[16,1024,2]{1,2,0:T(2,128)} %broadcast_in_dim.53), calls=%async_computation.2 | async-start | bytes 262144 | tf_op jit(solution)/shard_map/all_to_all | solution.py:22
  32.3 5.4 %all-to-all-done.2 = f32[16,1024,2]{1,2,0:T(2,128)S(1)} async-done(((f32[16,1024,2]{1,2,0:T(2,128)}), f32[16,1024,2]{1,2,0:T(2,128)S(1)}, u32[]{:S(2)}, u32[]{:S(2)}) %all-to-all-start.2) | async-done | bytes 131104 | tf_op jit(solution)/shard_map/all_to_all | solution.py:22
  37.7 2.5 stack.2
  40.1 6.6 %all-to-all-start.1 = ((bf16[16,1024,128]{1,2,0:T(8,128)(2,1)}), bf16[16,1024,128]{1,2,0:T(8,128)(2,1)}, u32[]{:S(2)}, u32[]{:S(2)}) async-start(bf16[16,1024,128]{1,2,0:T(8,128)(2,1)} %stack.2), calls=%async_computation.1 | async-start | bytes 8388608 | tf_op jit(solution)/shard_map/all_to_all | solution.py:158
  47.8 59.3 %collective-permute-done = bf16[512,2,64]{0,2,1:T(8,128)(2,1)S(1)} collective-permute-done((bf16[512,2,64]{0,2,1:T(8,128)(2,1)S(1)}, bf16[512,2,64]{0,2,1:T(8,128)(2,1)S(1)}, u32[]{:S(2)}, u32[]{:S(2)}) %collective-permute-start) | collective-permute-done | bytes 131104 | tf_op jit(solution)/shard_map/ppermute | solution.py:32
  107.1 6.5 %collective-permute-done.1 = bf16[512,2,64]{0,2,1:T(8,128)(2,1)S(1)} collective-permute-done((bf16[512,2,64]{0,2,1:T(8,128)(2,1)S(1)}, bf16[512,2,64]{0,2,1:T(8,128)(2,1)S(1)}, u32[]{:S(2)}, u32[]{:S(2)}) %collective-permute-start.1) | collective-permute-done | bytes 131104 | tf_op jit(solution)/shard_map/ppermute | solution.py:32
  113.6 5.0 %collective-permute-done.2 = bf16[512,2,64]{0,2,1:T(8,128)(2,1)S(1)} collective-permute-done((bf16[512,2,64]{0,2,1:T(8,128)(2,1)S(1)}, bf16[512,2,64]{0,2,1:T(8,128)(2,1)S(1)}, u32[]{:S(2)}, u32[]{:S(2)}) %collective-permute-start.2) | collective-permute-done | bytes 131104 | tf_op jit(solution)/shard_map/ppermute | solution.py:32
  118.5 3.2 %collective-permute-start.3 = (bf16[512,2,64]{0,2,1:T(8,128)(2,1)S(1)}, bf16[512,2,64]{0,2,1:T(8,128)(2,1)S(1)}, u32[]{:S(2)}, u32[]{:S(2)}) collective-permute-start(bf16[512,2,64]{0,2,1:T(8,128)(2,1)S(1)} %collective-permute-done.2), channel_id=1, source_target_pairs={{0,64},{8,72},{16,80},{24,88},{32,96},{40,104},{48,112},{56,120},{... | collective-permute-start | bytes 393224 | tf_op jit(solution)/shard_map/ppermute | solution.py:32
  121.8 6.4 %copy.70 = bf16[16,1024,128]{2,1,0:T(8,128)(2,1)} copy(bf16[16,1024,128]{1,2,0:T(8,128)(2,1)} %all-to-all-done.1) | data formatting | bytes 8388608 | tf_op jit(solution)/shard_map/all_to_all | solution.py:158
  128.3 133.0 %while.26 = (s32[]{:T(128)}, f32[2,512]{1,0:T(2,128)S(1)}, f32[2,512]{1,0:T(2,128)S(1)}, f32[512,2,64]{0,2,1:T(8,128)S(1)}, f32[2,512]{1,0:T(2,128)S(1)}, /*inde...) while((s32[]{:T(128)}, f32[2,512]{1,0:T(2,128)S(1)}, ...), condition=%wide.region_18.19_spmd.clone.clone, body=%wide.region_3.18_spmd.clone.clone.sunk | while | flops 280763904 | bytes 16956256 | solution.py:202
  131.0 1.4 conditional.9
  165.1 2.1 conditional.8
  243.0 2.1 conditional.9
  261.5 5.0 %collective-permute-done.4 = bf16[512,2,64]{0,2,1:T(8,128)(2,1)S(1)} collective-permute-done((bf16[512,2,64]{0,2,1:T(8,128)(2,1)S(1)}, bf16[512,2,64]{0,2,1:T(8,128)(2,1)S(1)}, u32[]{:S(2)}, u32[]{:S(2)}) %collective-permute-start.4) | collective-permute-done | bytes 131104 | tf_op jit(solution)/shard_map/ppermute | solution.py:32
  266.8 6.1 %collective-permute-done.5 = bf16[512,2,64]{0,2,1:T(8,128)(2,1)S(1)} collective-permute-done((bf16[512,2,64]{0,2,1:T(8,128)(2,1)S(1)}, bf16[512,2,64]{0,2,1:T(8,128)(2,1)S(1)}, u32[]{:S(2)}, u32[]{:S(2)}) %collective-permute-start.5) | collective-permute-done | bytes 131104 | tf_op jit(solution)/shard_map/ppermute | solution.py:32
  272.9 5.0 %collective-permute-done.6 = bf16[512,2,64]{0,2,1:T(8,128)(2,1)S(1)} collective-permute-done((bf16[512,2,64]{0,2,1:T(8,128)(2,1)S(1)}, bf16[512,2,64]{0,2,1:T(8,128)(2,1)S(1)}, u32[]{:S(2)}, u32[]{:S(2)}) %collective-permute-start.6) | collective-permute-done | bytes 131104 | tf_op jit(solution)/shard_map/ppermute | solution.py:32
  278.3 6.1 %collective-permute-done.7 = bf16[512,2,64]{0,2,1:T(8,128)(2,1)S(1)} collective-permute-done((bf16[512,2,64]{0,2,1:T(8,128)(2,1)S(1)}, bf16[512,2,64]{0,2,1:T(8,128)(2,1)S(1)}, u32[]{:S(2)}, u32[]{:S(2)}) %collective-permute-start.7) | collective-permute-done | bytes 131104 | tf_op jit(solution)/shard_map/ppermute | solution.py:32
  284.6 3.9 %all_to_all.36 = bf16[4,2,128,128]{2,3,0,1:T(8,128)(2,1)S(1)} all-to-all(bf16[4,2,128,128]{2,3,0,1:T(8,128)(2,1)S(1)} %copy.74), channel_id=1, replica_groups=mesh['sp'=16,'tp_0'=4,'tp_1'=2] {'tp_1'}, dimensions={1} | all-to-all | bytes 524288 | tf_op jit(solution)/shard_map/all_to_all | solution.py:44
  288.6 9.6 %all_to_all.37 = bf16[4,2,128,128]{2,3,1,0:T(8,128)(2,1)S(1)} all-to-all(bf16[4,2,128,128]{2,3,1,0:T(8,128)(2,1)S(1)} %copy.75), channel_id=1, replica_groups=mesh['sp'=16,'tp_0'=4,'tp_1'=2] {'tp_0'}, dimensions={0} | all-to-all | bytes 524288 | tf_op jit(solution)/shard_map/all_to_all | solution.py:44
  298.2 3.7 %convolution_convert_fusion = bf16[128,2048]{1,0:T(8,128)(2,1)} fusion(bf16[128,1024]{0,1:T(8,128)(2,1)S(1)} %bitcast.135, bf16[1024,2048]{1,0:T(8,128)(2,1)} %param.25), kind=kOutput, calls=%fused_computation.69 | convolution fusion | flops 537133056 | bytes 4980736 | tf_op jit(solution)/shard_map/dot_general | solution.py:211
  (576 shorter events, 155.1 us)
Async XLA Ops:
  0.0 1.3 copy-start
  0.0 4.4 %copy-start.1 = (bf16[128,2048]{1,0:T(8,128)(2,1)S(1)}, bf16[128,2048]{1,0:T(8,128)(2,1)}, u32[]{:S(2)}) copy-start(bf16[128,2048]{1,0:T(8,128)(2,1)} %param.17) | copy-start | bytes 1572868
  0.0 4.5 %copy-start.2 = (f32[2048]{0:T(1024)S(1)}, f32[2048]{0:T(1024)}, u32[]{:S(2)}) copy-start(f32[2048]{0:T(1024)} %param.18) | copy-start | bytes 24580
  7.4 0.7 copy-start.5
  7.4 0.7 copy-start.4
  8.3 14.7 %copy-start.3 = (f32[1024,2]{0,1:T(2,128)S(1)}, f32[1024,2]{0,1:T(2,128)}, u32[]{:S(2)}) copy-start(f32[1024,2]{0,1:T(2,128)} %param.24) | copy-start | bytes 24580
  23.7 14.0 %all-to-all-start.2 = ((f32[16,1024,2]{1,2,0:T(2,128)}), f32[16,1024,2]{1,2,0:T(2,128)S(1)}, u32[]{:S(2)}, u32[]{:S(2)}) async-start(f32[16,1024,2]{1,2,0:T(2,128)} %broadcast_in_dim.53), calls=%async_computation.2 | async-start | bytes 262144 | tf_op jit(solution)/shard_map/all_to_all | solution.py:22
  40.1 81.7 %all-to-all-start.1 = ((bf16[16,1024,128]{1,2,0:T(8,128)(2,1)}), bf16[16,1024,128]{1,2,0:T(8,128)(2,1)}, u32[]{:S(2)}, u32[]{:S(2)}) async-start(bf16[16,1024,128]{1,2,0:T(8,128)(2,1)} %stack.2), calls=%async_computation.1 | async-start | bytes 8388608 | tf_op jit(solution)/shard_map/all_to_all | solution.py:158
  46.9 60.2 %collective-permute-start = (bf16[512,2,64]{0,2,1:T(8,128)(2,1)S(1)}, bf16[512,2,64]{0,2,1:T(8,128)(2,1)S(1)}, u32[]{:S(2)}, u32[]{:S(2)}) collective-permute-start(bf16[512,2,64]{0,2,1:T(8,128)(2,1)S(1)} %bitcast.141), channel_id=1, source_target_pairs={{0,8},{8,0},{16,24},{24,16},{32,40},{40,32},{48,56},{56,48},{64,72... | collective-permute-start | bytes 393224 | tf_op jit(solution)/shard_map/ppermute | solution.py:32
  107.1 6.5 %collective-permute-start.1 = (bf16[512,2,64]{0,2,1:T(8,128)(2,1)S(1)}, bf16[512,2,64]{0,2,1:T(8,128)(2,1)S(1)}, u32[]{:S(2)}, u32[]{:S(2)}) collective-permute-start(bf16[512,2,64]{0,2,1:T(8,128)(2,1)S(1)} %collective-permute-done), channel_id=1, source_target_pairs={{0,16},{8,24},{16,0},{24,8},{32,48},{40,56},{48,32},{56,40},{64,80... | collective-permute-start | bytes 393224 | tf_op jit(solution)/shard_map/ppermute | solution.py:32
  113.6 5.0 %collective-permute-start.2 = (bf16[512,2,64]{0,2,1:T(8,128)(2,1)S(1)}, bf16[512,2,64]{0,2,1:T(8,128)(2,1)S(1)}, u32[]{:S(2)}, u32[]{:S(2)}) collective-permute-start(bf16[512,2,64]{0,2,1:T(8,128)(2,1)S(1)} %collective-permute-done.1), channel_id=1, source_target_pairs={{0,32},{8,40},{16,48},{24,56},{32,0},{40,8},{48,16},{56,24},{64,96... | collective-permute-start | bytes 393224 | tf_op jit(solution)/shard_map/ppermute | solution.py:32
  118.5 9.7 %collective-permute-start.3 = (bf16[512,2,64]{0,2,1:T(8,128)(2,1)S(1)}, bf16[512,2,64]{0,2,1:T(8,128)(2,1)S(1)}, u32[]{:S(2)}, u32[]{:S(2)}) collective-permute-start(bf16[512,2,64]{0,2,1:T(8,128)(2,1)S(1)} %collective-permute-done.2), channel_id=1, source_target_pairs={{0,64},{8,72},{16,80},{24,88},{32,96},{40,104},{48,112},{56,120},{... | collective-permute-start | bytes 393224 | tf_op jit(solution)/shard_map/ppermute | solution.py:32
  261.4 5.0 %collective-permute-start.4 = (bf16[512,2,64]{0,2,1:T(8,128)(2,1)S(1)}, bf16[512,2,64]{0,2,1:T(8,128)(2,1)S(1)}, u32[]{:S(2)}, u32[]{:S(2)}) collective-permute-start(bf16[512,2,64]{0,2,1:T(8,128)(2,1)S(1)} %divide_convert_fusion), channel_id=1, source_target_pairs={{0,8},{8,0},{16,24},{24,16},{32,40},{40,32},{48,56},{56,48},{64,72... | collective-permute-start | bytes 393224 | tf_op jit(solution)/shard_map/ppermute | solution.py:32
  266.5 6.5 %collective-permute-start.5 = (bf16[512,2,64]{0,2,1:T(8,128)(2,1)S(1)}, bf16[512,2,64]{0,2,1:T(8,128)(2,1)S(1)}, u32[]{:S(2)}, u32[]{:S(2)}) collective-permute-start(bf16[512,2,64]{0,2,1:T(8,128)(2,1)S(1)} %collective-permute-done.4), channel_id=1, source_target_pairs={{0,16},{8,24},{16,0},{24,8},{32,48},{40,56},{48,32},{56,40},{64,80... | collective-permute-start | bytes 393224 | tf_op jit(solution)/shard_map/ppermute | solution.py:32
  272.9 5.0 %collective-permute-start.6 = (bf16[512,2,64]{0,2,1:T(8,128)(2,1)S(1)}, bf16[512,2,64]{0,2,1:T(8,128)(2,1)S(1)}, u32[]{:S(2)}, u32[]{:S(2)}) collective-permute-start(bf16[512,2,64]{0,2,1:T(8,128)(2,1)S(1)} %collective-permute-done.5), channel_id=1, source_target_pairs={{0,32},{8,40},{16,48},{24,56},{32,0},{40,8},{48,16},{56,24},{64,96... | collective-permute-start | bytes 393224 | tf_op jit(solution)/shard_map/ppermute | solution.py:32
  277.9 6.5 %collective-permute-start.7 = (bf16[512,2,64]{0,2,1:T(8,128)(2,1)S(1)}, bf16[512,2,64]{0,2,1:T(8,128)(2,1)S(1)}, u32[]{:S(2)}, u32[]{:S(2)}) collective-permute-start(bf16[512,2,64]{0,2,1:T(8,128)(2,1)S(1)} %collective-permute-done.6), channel_id=1, source_target_pairs={{0,64},{8,72},{16,80},{24,88},{32,96},{40,104},{48,112},{56,120},{... | collective-permute-start | bytes 393224 | tf_op jit(solution)/shard_map/ppermute | solution.py:32
